TPU v7x, 32 devices: a whole 2x2x4 slice. The times are simulated.
32 devices in a mesh: sp: 16 (over z, y, x), tp: 2 (over core).
Axes of the slice: x: 2, y: 2, z: 4, core: 2. Of those that a mesh axis runs over, the one named last changes fastest.
Arguments:
- proj_a: bfloat16 [4096, 3072], P('sp', 'tp'), may hold values from -20 to 20
- proj_gate: bfloat16 [4096, 3072], P('sp', 'tp'), may hold values from -6 to 6
- taps: bfloat16 [31, 3072], P(None, 'tp'), may hold values from -1 to 1
- norm_gain: float32 [3072], P('tp'), may hold values from 0.1 to 1.9
- norm_shift: float32 [3072], P('tp'), may hold values from -3 to 3
- cotangent: bfloat16 [4096, 3072], P('sp', 'tp'), may hold values from -6 to 6
Outputs:
- a_grad: bfloat16 [4096, 3072], P('sp', 'tp')
- gate_grad: bfloat16 [4096, 3072], P('sp', 'tp')
- taps_grad: float32 [31, 3072], P(None, 'tp')
- gain_grad: float32 [3072], P('tp')
- shift_grad: float32 [3072], P('tp')
All inputs are finite; a program needn't handle non-finite values.
Results may differ from a plain program's by a relative error of at most 0.0048.
Values may be sent and summed in bfloat16 or wider, within the bound.
A program may use at most 64 MiB of HBM per device.

v0:
```python
import functools

import jax
import jax.numpy as jnp
from jax import lax
from jax.experimental import pallas as pl
from jax.experimental.pallas import tpu as pltpu
from jax.sharding import PartitionSpec as P

EPS = 1e-05
LANES = 128
SUB = 8
BLOCK = 64
HALO = 32
F32 = jnp.float32
BF16 = jnp.bfloat16


PACK = 16


def plan(chans, width, n):
    tiles = chans // LANES
    rounds = 2 if tiles % 2 == 0 else 1
    group = -(-(width + 2) // SUB) * SUB
    total = tiles // rounds * group
    chunk = -(-total // (n * PACK)) * PACK
    owners = -(-total // chunk)
    return tiles, rounds, group, chunk, owners


def kernel(
    n, ntp, width, full,
    a_hbm, g_hbm, taps_hbm, gain_ref, shift_ref, cot_hbm,
    ag_ref, gg_ref, sums_ref,
    a_ref, g_ref, cot_ref, taps_ref, x_s, conv_s, dn_s, d_s, taps_s, par_s,
    glu_out, glu_in, dc_out, dc_in,
    st_out, st_in, stat_s,
    red_f, red_s, rs_in, ag_src, ag_in, in_sem,
    halo_send, halo_recv, st_send, st_recv,
    rs_send, rs_recv, ag_send, ag_recv,
):
    rows, chans = a_hbm.shape
    edge = width - 1
    lead = HALO - edge
    tiles, rounds, group, chunk, owners = plan(chans, width, n)
    part_tiles = tiles // rounds
    blocks = rows // BLOCK
    tail, body = pl.ds(rows - HALO, HALO), pl.ds(0, rows - HALO)
    loads = [
        pltpu.make_async_copy(src, dst, in_sem.at[i])
        for i, (src, dst) in enumerate((
            (g_hbm.at[tail, :], g_ref.at[tail, :]),
            (a_hbm.at[tail, :], a_ref.at[tail, :]),
            (g_hbm.at[body, :], g_ref.at[body, :]),
            (a_hbm.at[body, :], a_ref.at[body, :]),
            (taps_hbm, taps_ref),
            (cot_hbm, cot_ref),
        ))
    ]
    for load in loads:
        load.start()
    me = lax.axis_index("sp")
    core = lax.axis_index("tp")
    other = 1 - core

    barrier = pltpu.get_barrier_semaphore()

    def greet(step, carry):
        pl.semaphore_signal(barrier, inc=1, device_id={"sp": lax.rem(me + step, n)})
        return carry

    lax.fori_loop(1, n, greet, 0)
    pl.semaphore_signal(barrier, inc=1, device_id={"tp": other})

    def cols(j):
        return pl.ds(pl.multiple_of(j * LANES, LANES), LANES)

    def gate_tile(j, base, count):
        a = a_ref[pl.ds(base, count), cols(j)].astype(F32)
        g = g_ref[pl.ds(base, count), cols(j)].astype(F32)
        return (a * jax.nn.sigmoid(g)).astype(BF16)

    def last_rows(j, carry):
        glu_out[j] = gate_tile(j, rows - HALO, HALO)
        return carry

    loads[0].wait()
    loads[1].wait()
    lax.fori_loop(0, tiles, last_rows, 0)

    glu_copy = pltpu.make_async_remote_copy(
        src_ref=glu_out, dst_ref=glu_in, send_sem=halo_send.at[0], recv_sem=halo_recv.at[0],
        device_id={"sp": lax.rem(me + 1, n)},
    )
    dc_copy = pltpu.make_async_remote_copy(
        src_ref=dc_out, dst_ref=dc_in, send_sem=halo_send.at[1], recv_sem=halo_recv.at[1],
        device_id={"sp": lax.rem(me + n - 1, n)},
    )

    def prepare(j, carry):
        taps_s[j, pl.ds(0, width), :] = taps_ref[:, cols(j)].astype(F32)
        par_s[j, 0:1, :] = gain_ref[cols(j)].reshape(1, LANES)
        par_s[j, 1:2, :] = shift_ref[cols(j)].reshape(1, LANES)
        par_s[j, pl.ds(SUB, 2 * SUB), :] = jnp.zeros((2 * SUB, LANES), F32)
        for b in range(blocks):
            x_s[j, pl.ds(HALO + b * BLOCK, BLOCK), :] = gate_tile(j, b * BLOCK, BLOCK).astype(F32)
        return carry

    for load in loads[2:5]:
        load.wait()
    pl.semaphore_wait(barrier, n)

    @pl.when(me < n - 1)
    def _():
        glu_copy.start()

    lax.fori_loop(0, tiles, prepare, 0)

    lane = lax.broadcasted_iota(jnp.int32, (BLOCK, LANES), 1)

    def stat_copy(i):
        return pltpu.make_async_remote_copy(
            src_ref=st_out.at[i], dst_ref=st_in.at[i], send_sem=st_send.at[i],
            recv_sem=st_recv.at[i], device_id={"tp": other},
        )

    def send_stats(i, first, second):
        first = jnp.sum(first, axis=1, keepdims=True)
        second = jnp.sum(second, axis=1, keepdims=True)
        st_out[i] = jnp.where(lane < LANES // 2, first, second)
        stat_copy(i).start()

    def both_stats(i):
        stat_copy(i).wait_recv()
        both = (st_out[i] + st_in[i]) * (1.0 / full)
        first = jnp.broadcast_to(both[:, 0:1], (BLOCK, LANES))
        second = jnp.broadcast_to(both[:, LANES // 2 : LANES // 2 + 1], (BLOCK, LANES))
        return first, second

    zero = jnp.zeros((BLOCK, LANES), F32)

    def convolve(b):
        base = b * BLOCK

        def step(j, carry):
            first, second = carry
            acc = zero
            for k in range(width):
                acc = acc + taps_s[j, k : k + 1, :] * x_s[j, pl.ds(base + lead + k, BLOCK), :]
            conv_s[j, pl.ds(base, BLOCK), :] = acc
            return first + acc, second + acc * acc

        first, second = lax.fori_loop(0, tiles, step, (zero, zero))
        send_stats(b, first, second)

    def fold(x):
        return jnp.sum(x.reshape(x.shape[0] // SUB, SUB, LANES), axis=0)

    def normalise(b):
        base = b * BLOCK
        mean, square = both_stats(b)
        rstd = lax.rsqrt(jnp.maximum(square - mean * mean, 0.0) + EPS)
        stat_s[0, pl.ds(base, BLOCK), :] = rstd

        def step(j, carry):
            first, second = carry
            at = pl.ds(base, BLOCK)
            gain = par_s[j, 0:1, :]
            normed = (conv_s[j, at, :] - mean) * rstd
            pre = normed * gain + par_s[j, 1:2, :]
            sig = jax.nn.sigmoid(pre)
            dpre = cot_ref[at, cols(j)].astype(F32) * sig * (1.0 + pre * (1.0 - sig))
            par_s[j, pl.ds(SUB, SUB), :] += fold(dpre * normed)
            par_s[j, pl.ds(2 * SUB, SUB), :] += fold(dpre)
            dn = dpre * gain
            conv_s[j, at, :] = normed
            dn_s[j, at, :] = dn
            return first + dn, second + dn * normed

        first, second = lax.fori_loop(0, tiles, step, (zero, zero))
        send_stats(blocks + b, first, second)

    def take_stats(b):
        first, second = both_stats(blocks + b)
        at = pl.ds(b * BLOCK, BLOCK)
        stat_s[1, at, :] = first
        stat_s[2, at, :] = second

    def dconv_at(j, at):
        return stat_s[0, at, :] * (
            dn_s[j, at, :] - stat_s[1, at, :] - conv_s[j, at, :] * stat_s[2, at, :]
        )

    for b in range(1, blocks):
        convolve(b)
    loads[5].wait()
    for b in range(1, blocks):
        normalise(b)

    @pl.when(me > 0)
    def _():
        glu_copy.wait_recv()

        def widen(j, carry):
            x_s[j, pl.ds(0, HALO), :] = glu_in[j].astype(F32)
            return carry

        lax.fori_loop(0, tiles, widen, 0)

    @pl.when(me == 0)
    def _():
        def clear(j, carry):
            x_s[j, pl.ds(0, HALO), :] = jnp.zeros((HALO, LANES), F32)
            return carry

        lax.fori_loop(0, tiles, clear, 0)

    convolve(0)
    for b in range(1, blocks):
        take_stats(b)
    normalise(0)
    take_stats(0)

    def head(j, carry):
        dc_out[j] = dconv_at(j, pl.ds(0, HALO)).astype(BF16)
        return carry

    lax.fori_loop(0, tiles, head, 0)

    @pl.when(me > 0)
    def _():
        dc_copy.start()

    spare = owners * chunk - part_tiles * group

    def taps_round(h):
        def step(i, carry):
            j = h * part_tiles + i
            d = dconv_at(j, pl.ds(0, rows))
            d_s[j, pl.ds(0, rows), :] = d
            at = pl.multiple_of(i * group, SUB)
            for k in range(width):
                prod = d * x_s[j, pl.ds(lead + k, rows), :]
                red_f[pl.ds(at + k, 1), :] = jnp.sum(prod, axis=0, keepdims=True)
            for k in range(2):
                red_f[pl.ds(at + width + k, 1), :] = jnp.sum(
                    par_s[j, pl.ds(SUB + k * SUB, SUB), :], axis=0, keepdims=True
                )
            for k in range(width + 2, group):
                red_f[pl.ds(at + k, 1), :] = jnp.zeros((1, LANES), F32)
            return carry

        lax.fori_loop(0, part_tiles, step, 0)
        if spare:
            red_f[pl.ds(part_tiles * group, spare), :] = jnp.zeros((spare, LANES), F32)
        red_s[h] = red_f[...].astype(BF16)

    def part(owner):
        return pl.ds(pl.multiple_of(owner * chunk, PACK), chunk)

    def rs_copy(h, owner, source, to):
        return pltpu.make_async_remote_copy(
            src_ref=red_s.at[h, part(owner), :], dst_ref=rs_in.at[h, source],
            send_sem=rs_send.at[h * n + owner], recv_sem=rs_recv.at[h * n + source],
            device_id={"sp": to},
        )

    def ag_copy(h, owner, to):
        return pltpu.make_async_remote_copy(
            src_ref=ag_src.at[h], dst_ref=ag_in.at[h, part(owner), :],
            send_sem=ag_send.at[h * n + to], recv_sem=ag_recv.at[h * n + owner],
            device_id={"sp": to},
        )

    def peers(run, limit=n):
        def step(d, carry):
            peer = lax.rem(me + d, n)
            if limit == n:
                run(peer)
            else:
                pl.when(peer < limit)(lambda: run(peer))
            return carry

        lax.fori_loop(1, n, step, 0)

    def scatter(h):
        peers(lambda peer: rs_copy(h, peer, me, peer).start(), owners)

    def gather(h):
        @pl.when(me < owners)
        def _():
            rs_in[h, me] = red_s[h, part(me), :]
            peers(lambda peer: rs_copy(h, me, peer, peer).wait_recv())
            ag_src[h] = lax.fori_loop(
                1, n, lambda s, total: total + rs_in[h, s].astype(F32), rs_in[h, 0].astype(F32)
            ).astype(BF16)
            peers(lambda peer: ag_copy(h, me, peer).start())
            ag_in[h, part(me), :] = ag_src[h]

    for h in range(rounds):
        taps_round(h)
        scatter(h)

    def back(b):
        base = b * BLOCK

        def step(j, carry):
            acc = zero
            for k in range(width):
                acc = acc + taps_s[j, edge - k : edge - k + 1, :] * d_s[j, pl.ds(base + k, BLOCK), :]
            at = pl.ds(base, BLOCK)
            sg = jax.nn.sigmoid(g_ref[at, cols(j)].astype(F32))
            first = acc * sg
            ag_ref[at, cols(j)] = first.astype(BF16)
            gg_ref[at, cols(j)] = (first * a_ref[at, cols(j)].astype(F32) * (1.0 - sg)).astype(BF16)
            return carry

        lax.fori_loop(0, tiles, step, 0)

    back(0)
    for h in range(rounds - 1):
        gather(h)
    for b in range(1, blocks - 1):
        back(b)

    @pl.when(me < n - 1)
    def _():
        dc_copy.wait_recv()

        def widen(j, carry):
            d_s[j, pl.ds(rows, HALO), :] = dc_in[j].astype(F32)
            return carry

        lax.fori_loop(0, tiles, widen, 0)

    @pl.when(me == n - 1)
    def _():
        def clear(j, carry):
            d_s[j, pl.ds(rows, HALO), :] = jnp.zeros((HALO, LANES), F32)
            return carry

        lax.fori_loop(0, tiles, clear, 0)

    back(blocks - 1)
    gather(rounds - 1)

    for h in range(rounds):
        peers(lambda peer: rs_copy(h, peer, me, peer).wait_send(), owners)

    @pl.when(me < n - 1)
    def _():
        glu_copy.wait_send()

    @pl.when(me > 0)
    def _():
        dc_copy.wait_send()

    for i in range(2 * blocks):
        stat_copy(i).wait_send()

    for h in range(rounds):
        peers(lambda peer: ag_copy(h, peer, peer).wait_recv(), owners)
        sums_ref[h] = ag_in[h].astype(F32)

    @pl.when(me < owners)
    def _():
        for h in range(rounds):
            peers(lambda peer: ag_copy(h, me, peer).wait_send())


def finish(width, part_tiles, group, ag_ref, gg_ref, sums_ref, ag_out, gg_out, tg_ref, gaing_ref, shiftg_ref, sems):
    first = pltpu.make_async_copy(ag_ref, ag_out, sems.at[0])
    second = pltpu.make_async_copy(gg_ref, gg_out, sems.at[1])
    first.start()
    second.start()
    for h in range(sums_ref.shape[0]):
        for i in range(part_tiles):
            at = pl.ds((h * part_tiles + i) * LANES, LANES)
            tg_ref[:, at] = sums_ref[h, pl.ds(i * group, width), :]
            gaing_ref[at] = sums_ref[h, i * group + width, :]
            shiftg_ref[at] = sums_ref[h, i * group + width + 1, :]
    first.wait()
    second.wait()


def solution(mesh):
    n, ntp = mesh.shape["sp"], mesh.shape["tp"]

    def body(proj_a, proj_gate, taps, norm_gain, norm_shift, cotangent):
        rows, chans = proj_a.shape
        width = taps.shape[0]
        tiles, rounds, group, chunk, owners = plan(chans, width, n)
        blocks = rows // BLOCK
        vmem = pl.BlockSpec(memory_space=pltpu.VMEM)
        hbm = pl.BlockSpec(memory_space=pltpu.HBM)
        wide = jax.ShapeDtypeStruct((rows, chans), BF16)
        a_grad, gate_grad, sums = pl.pallas_call(
            functools.partial(kernel, n, ntp, width, chans * ntp),
            out_shape=(wide, wide, jax.ShapeDtypeStruct((rounds, owners * chunk, LANES), F32)),
            in_specs=[hbm, hbm, hbm, vmem, vmem, hbm],
            out_specs=(vmem,) * 3,
            scratch_shapes=[
                pltpu.VMEM((rows, chans), BF16),
                pltpu.VMEM((rows, chans), BF16),
                pltpu.VMEM((rows, chans), BF16),
                pltpu.VMEM((width, chans), BF16),
                pltpu.VMEM((tiles, HALO + rows, LANES), F32),
                pltpu.VMEM((tiles, rows, LANES), F32),
                pltpu.VMEM((tiles, rows, LANES), F32),
                pltpu.VMEM((tiles, rows + HALO, LANES), F32),
                pltpu.VMEM((tiles, -(-width // SUB) * SUB, LANES), F32),
                pltpu.VMEM((tiles, 3 * SUB, LANES), F32),
                pltpu.VMEM((tiles, HALO, LANES), BF16),
                pltpu.VMEM((tiles, HALO, LANES), BF16),
                pltpu.VMEM((tiles, HALO, LANES), BF16),
                pltpu.VMEM((tiles, HALO, LANES), BF16),
                pltpu.VMEM((2 * blocks, BLOCK, LANES), F32),
                pltpu.VMEM((2 * blocks, BLOCK, LANES), F32),
                pltpu.VMEM((3, rows, LANES), F32),
                pltpu.VMEM((owners * chunk, LANES), F32),
                pltpu.VMEM((rounds, owners * chunk, LANES), BF16),
                pltpu.VMEM((rounds, n, chunk, LANES), BF16),
                pltpu.VMEM((rounds, chunk, LANES), BF16),
                pltpu.VMEM((rounds, owners * chunk, LANES), BF16),
                pltpu.SemaphoreType.DMA((6,)),
                pltpu.SemaphoreType.DMA((2,)),
                pltpu.SemaphoreType.DMA((2,)),
                pltpu.SemaphoreType.DMA((2 * blocks,)),
                pltpu.SemaphoreType.DMA((2 * blocks,)),
                pltpu.SemaphoreType.DMA((rounds * n,)),
                pltpu.SemaphoreType.DMA((rounds * n,)),
                pltpu.SemaphoreType.DMA((rounds * n,)),
                pltpu.SemaphoreType.DMA((rounds * n,)),
            ],
            compiler_params=pltpu.CompilerParams(
                collective_id=0, has_side_effects=True, vmem_limit_bytes=32 * 1024 * 1024
            ),
        )(*(
            pltpu.with_memory_space_constraint(x, pltpu.HBM)
            for x in (proj_a, proj_gate, taps, norm_gain, norm_shift, cotangent)
        ))
        vector = jax.ShapeDtypeStruct((chans,), F32)
        return pl.pallas_call(
            functools.partial(finish, width, tiles // rounds, group),
            out_shape=(wide, wide, jax.ShapeDtypeStruct((width, chans), F32), vector, vector),
            in_specs=[vmem] * 3,
            out_specs=(hbm, hbm, vmem, vmem, vmem),
            scratch_shapes=[pltpu.SemaphoreType.DMA((2,))],
            compiler_params=pltpu.CompilerParams(vmem_limit_bytes=16 * 1024 * 1024),
        )(a_grad, gate_grad, sums)

    placed = (P("sp", "tp"), P("sp", "tp"), P(None, "tp"), P("tp"), P("tp"), P("sp", "tp"))
    return jax.shard_map(
        body,
        mesh=mesh,
        in_specs=placed,
        out_specs=(P("sp", "tp"), P("sp", "tp"), P(None, "tp"), P("tp"), P("tp")),
        check_vma=False,
    )
```

profile of v0, /device:TPU:0, one launch (start us, length us, event | category | flops | bytes accessed | tf_op | source)
XLA Modules:
  0.0 35.2 jit_solution(8808627965042767567)
XLA Ops:
  0.6 32.7 %shard_map.101 = (bf16[256,1536]{1,0:T(8,128)(2,1)S(1)}, bf16[256,1536]{1,0:T(8,128)(2,1)S(1)}, f32[2,240,128]{2,1,0:T(8,128)S(1)}) custom-call(bf16[256,1536]{1,0:T(8,128)(2,1)} %a_hbm.1, bf16[256,1536]{1,0:T(8,128)(2,1)} %g_hbm.1, bf16[31,1536]{1,0:T(8,128)(2,1)} %taps_hbm.1, f32[1536]{0:T(1024)} %gain_ref.1, f32[1536]{0:T(1024)} %shift_ref.1, ...), custom_call_target="tpu_custom_call" | custom-call | tf_op jit(solution)/shard_map/pallas_call | solution.py:398
  33.4 1.8 %shard_map.102 = (bf16[256,1536]{1,0:T(8,128)(2,1)}, bf16[256,1536]{1,0:T(8,128)(2,1)}, f32[31,1536]{1,0:T(8,128)}, f32[1536]{0:T(1024)}, f32[1536]{0:T(1024)}) custom-call(bf16[256,1536]{1,0:T(8,128)(2,1)S(1)} %get-tuple-element.8.ag_ref, bf16[256,1536]{1,0:T(8,128)(2,1)S(1)} %get-tuple-element.9.gg_ref, f32[2,240,128]{2,1,0:T(8,128)S(1)} %get-tuple-element.10.sums_ref), custom_call_target="tpu_custom_call" | custom-call | tf_op jit(solution)/shard_map/pallas_call | solution.py:444
where the time goes:
time: 35.5 us; the launch traced here: 35.2 us
  Pallas kernels  34.6 us (97%)
  between operations  0.64 us (2%)
    pallas_call x1, Pallas kernels, body(): pl.pallas_call(functools.partial(kernel, n, ntp, width, chans * ntp), out...  32.7 us
    pallas_call x1, Pallas kernels, body(): pl.pallas_call(functools.partial(finish, width, tiles // rounds, group),...  1.84 us

commit v1 on v0

v1 whole, which is shorter than its diff:
```python
import functools

import jax
import jax.numpy as jnp
from jax import lax
from jax.experimental import pallas as pl
from jax.experimental.pallas import tpu as pltpu
from jax.sharding import PartitionSpec as P

EPS = 1e-05
LANES = 128
SUB = 8
PACK = 16
BLOCK = 64
HALO = 32
STEP = SUB + 1
F32 = jnp.float32
BF16 = jnp.bfloat16


def plan(chans, width, n):
    tiles = chans // LANES
    rounds = 2 if tiles % 2 == 0 else 1
    slots = -(-(width + 1) // SUB) * SUB
    total = tiles // rounds * (slots + 1)
    share = PACK * max(n // 2, 1)
    chunk = -(-total // share) * PACK
    owners = -(-total // chunk)
    return tiles, rounds, slots, chunk, owners, (n - owners) // 2


def products(pairs):
    total = None
    for x, y in pairs:
        prod = x.astype(F32) * y.astype(F32)
        total = prod if total is None else total + prod
    return total


def kernel(
    n, width, full,
    a_hbm, g_hbm, taps_hbm, gain_hbm, shift_hbm, cot_hbm,
    ag_ref, gg_ref, sums_ref,
    a_ref, g_ref, cot_ref, taps_ref, gain_ref, shift_ref,
    tap_s, x_s, xa_s, xb_s, conv_s, dn_s, d_s, d_t, da_s, db_s, par_s, part_s,
    glu_out, glu_in, dc_out, dc_in,
    st_out, st_in, stat_s,
    red_f, red_s, rs_in, ag_src, ag_in,
    in_sem, halo_send, halo_recv, st_send, st_recv,
    rs_send, rs_recv, ag_send, ag_recv,
):
    rows, chans = a_hbm.shape
    edge = width - 1
    lead = HALO - edge
    tiles, rounds, slots, chunk, owners, first_owner = plan(chans, width, n)
    part_tiles = tiles // rounds
    blocks = rows // BLOCK
    far, near = (rows - BLOCK) // PACK, BLOCK // PACK
    loads = [
        pltpu.make_async_copy(src, dst, in_sem.at[i])
        for i, (src, dst) in enumerate((
            (taps_hbm, taps_ref),
            (g_hbm, g_ref),
            (a_hbm, a_ref),
            (gain_hbm, gain_ref),
            (shift_hbm, shift_ref),
            (cot_hbm, cot_ref),
        ))
    ]
    for load in loads:
        load.start()
    me = lax.axis_index("sp")
    other = 1 - lax.axis_index("tp")

    barrier = pltpu.get_barrier_semaphore()

    def greet(step, carry):
        pl.semaphore_signal(barrier, inc=1, device_id={"sp": lax.rem(me + step, n)})
        return carry

    pl.semaphore_signal(barrier, inc=1, device_id={"tp": other})
    lax.fori_loop(1, n, greet, 0)

    def cols(j):
        return pl.ds(pl.multiple_of(j * LANES, LANES), LANES)

    def each_tile(run):
        def step(j, carry):
            run(j)
            return carry

        lax.fori_loop(0, tiles, step, 0)

    def over_tiles(run, carry, unroll):
        unroll = unroll if tiles % unroll == 0 else 1

        def step(i, carry):
            for u in range(unroll):
                carry = run(i * unroll + u, carry)
            return carry

        return lax.fori_loop(0, tiles // unroll, step, carry)

    glu_copy = pltpu.make_async_remote_copy(
        src_ref=glu_out, dst_ref=glu_in, send_sem=halo_send.at[0], recv_sem=halo_recv.at[0],
        device_id={"sp": lax.rem(me + 1, n)},
    )
    dc_copy = pltpu.make_async_remote_copy(
        src_ref=dc_out, dst_ref=dc_in, send_sem=halo_send.at[1], recv_sem=halo_recv.at[1],
        device_id={"sp": lax.rem(me + n - 1, n)},
    )

    def spread(src, dst, j, base, stride, count, at=0):
        for m in range(count):
            dst[j, at + m] = src[j, pl.ds(base + m, PACK, stride=stride), :].astype(BF16)

    def correlate(src, dst, j, base, stride, order):
        for m in range(stride):
            dst[j, pl.ds(base + m, PACK, stride=stride), :] = products(
                (src[j, m + i], tap_s[j, k]) for i, k in enumerate(order)
            )

    forward = range(width)
    backward = range(edge, -1, -1)

    def spread_taps(j):
        for k in range(width):
            row = taps_ref[pl.ds(k, 1), cols(j)].astype(F32)
            tap_s[j, k] = jnp.broadcast_to(row, (PACK, LANES)).astype(BF16)

    def gate_tile(j):
        for b in range(blocks):
            at = pl.ds(b * BLOCK, BLOCK)
            a = a_ref[at, cols(j)].astype(F32)
            g = g_ref[at, cols(j)].astype(F32)
            glu = (a * jax.nn.sigmoid(g)).astype(BF16)
            x_s[j, pl.ds(HALO + b * BLOCK, BLOCK), :] = glu.astype(F32)
            if b == blocks - 1:
                glu_out[j] = glu[BLOCK - HALO :]
        spread(x_s, xa_s, j, lead + BLOCK, far, far + edge)

    loads[0].wait()
    each_tile(spread_taps)
    loads[1].wait()
    loads[2].wait()
    each_tile(gate_tile)
    pl.semaphore_wait(barrier, n)

    @pl.when(me < n - 1)
    def _():
        glu_copy.start()

    each_tile(lambda j: correlate(xa_s, conv_s, j, BLOCK, far, forward))

    lane = lax.broadcasted_iota(jnp.int32, (BLOCK, LANES), 1)
    zero = jnp.zeros((BLOCK, LANES), F32)

    def stat_copy(i):
        return pltpu.make_async_remote_copy(
            src_ref=st_out.at[i], dst_ref=st_in.at[i], send_sem=st_send.at[i],
            recv_sem=st_recv.at[i], device_id={"tp": other},
        )

    def send_stats(i, first, second):
        first = jnp.sum(first, axis=1, keepdims=True)
        second = jnp.sum(second, axis=1, keepdims=True)
        st_out[i] = jnp.where(lane < LANES // 2, first, second)
        stat_copy(i).start()

    def both_stats(i):
        stat_copy(i).wait_recv()
        both = (st_out[i] + st_in[i]) * (1.0 / full)
        first = jnp.broadcast_to(both[:, 0:1], (BLOCK, LANES))
        second = jnp.broadcast_to(both[:, LANES // 2 : LANES // 2 + 1], (BLOCK, LANES))
        return first, second

    def moments(b):
        def step(j, carry):
            first, second = carry
            x = conv_s[j, pl.ds(b * BLOCK, BLOCK), :]
            return first + x, second + x * x

        send_stats(b, *over_tiles(step, (zero, zero), 3))

    def fold(x):
        return jnp.sum(x.reshape(x.shape[0] // SUB, SUB, LANES), axis=0)

    def normalise(b):
        at = pl.ds(b * BLOCK, BLOCK)
        mean, square = both_stats(b)
        rstd = lax.rsqrt(jnp.maximum(square - mean * mean, 0.0) + EPS)
        stat_s[at, :] = rstd

        def step(j, carry):
            first, second = carry
            gain = par_s[j, 0:1, :]
            normed = (conv_s[j, at, :] - mean) * rstd
            pre = normed * gain + par_s[j, 1:2, :]
            sig = jax.nn.sigmoid(pre)
            dpre = cot_ref[at, cols(j)].astype(F32) * sig * (1.0 + pre * (1.0 - sig))
            par_s[j, pl.ds(SUB, SUB), :] += fold(dpre * normed)
            par_s[j, pl.ds(2 * SUB, SUB), :] += fold(dpre)
            dn = dpre * gain
            conv_s[j, at, :] = normed
            dn_s[j, at, :] = dn
            return first + dn, second + dn * normed

        send_stats(blocks + b, *lax.fori_loop(0, tiles, step, (zero, zero)))

    def dconv(b):
        at = pl.ds(b * BLOCK, BLOCK)
        first, second = both_stats(blocks + b)
        rstd = stat_s[at, :]

        def step(j, carry):
            d_s[j, at, :] = rstd * (dn_s[j, at, :] - first - conv_s[j, at, :] * second)
            return carry

        over_tiles(step, 0, 2)

    for b in range(1, blocks):
        moments(b)

    loads[3].wait()
    loads[4].wait()

    def parameters(j):
        par_s[j, 0:1, :] = gain_ref[cols(j)].reshape(1, LANES)
        par_s[j, 1:2, :] = shift_ref[cols(j)].reshape(1, LANES)
        par_s[j, pl.ds(SUB, 2 * SUB), :] = jnp.zeros((2 * SUB, LANES), F32)

    each_tile(parameters)
    loads[5].wait()

    @pl.when(me > 0)
    def _():
        glu_copy.wait_recv()

        def widen(j):
            x_s[j, pl.ds(0, HALO), :] = glu_in[j].astype(F32)

        each_tile(widen)

    @pl.when(me == 0)
    def _():
        def clear(j):
            x_s[j, pl.ds(0, HALO), :] = jnp.zeros((HALO, LANES), F32)

        each_tile(clear)

    def near_tile(j):
        spread(x_s, xb_s, j, lead, near, near + edge)
        correlate(xb_s, conv_s, j, 0, near, forward)

    each_tile(near_tile)
    moments(0)
    order = (*range(1, blocks), 0)
    for b in order:
        normalise(b)
    for b in order:
        dconv(b)

    def head(j):
        dc_out[j] = d_s[j, pl.ds(0, HALO), :].astype(BF16)

    each_tile(head)

    @pl.when(me > 0)
    def _():
        dc_copy.start()

    spare = owners * chunk - part_tiles * (slots + 1)
    part_s[pl.ds(width * STEP, (slots - width) * STEP), :] = jnp.zeros(
        ((slots - width) * STEP, LANES), F32
    )

    def taps_round(h):
        def step(i, carry):
            j = h * part_tiles + i
            spread(d_s, d_t, j, BLOCK, far, far)
            spread(d_s, d_t, j, 0, near, near, far)
            for k in range(width):
                both = products(
                    [(xa_s[j, m + k], d_t[j, m]) for m in range(far)]
                    + [(xb_s[j, m + k], d_t[j, far + m]) for m in range(near)]
                )
                part_s[pl.ds(k * STEP, SUB), :] = both[:SUB] + both[SUB:]
            part_s[pl.ds(width * STEP, SUB), :] = par_s[j, pl.ds(SUB, SUB), :]
            for q in range(slots // SUB):
                total = part_s[pl.ds(q * SUB * STEP, SUB, stride=STEP), :]
                for r in range(1, SUB):
                    total = total + part_s[pl.ds(q * SUB * STEP + r, SUB, stride=STEP), :]
                red_f[pl.ds(pl.multiple_of(i * slots, SUB) + q * SUB, SUB), :] = total
            red_f[pl.ds(part_tiles * slots + i, 1), :] = jnp.sum(
                par_s[j, pl.ds(2 * SUB, SUB), :], axis=0, keepdims=True
            )
            return carry

        lax.fori_loop(0, part_tiles, step, 0)
        if spare:
            red_f[pl.ds(part_tiles * (slots + 1), spare), :] = jnp.zeros((spare, LANES), F32)
        red_s[h] = red_f[...].astype(BF16)

    mine = me - first_owner
    owner = jnp.logical_and(mine >= 0, mine < owners)

    def part(o):
        return pl.ds(pl.multiple_of(o * chunk, PACK), chunk)

    def bytes_of(ref, sem):
        return pltpu.make_async_copy(ref, ref, sem)

    def scatter(h):
        def step(i, carry):
            o = lax.rem(me + i, owners)
            to = first_owner + o

            @pl.when(to != me)
            def _():
                pltpu.make_async_remote_copy(
                    src_ref=red_s.at[h, part(o), :],
                    dst_ref=rs_in.at[h, lax.rem(me - to + n, n) - 1],
                    send_sem=rs_send.at[h], recv_sem=rs_recv.at[h], device_id={"sp": to},
                ).start()

            return carry

        lax.fori_loop(0, owners, step, 0)

    def gather(h):
        @pl.when(owner)
        def _():
            bytes_of(rs_in.at[h], rs_recv.at[h]).wait()
            ag_src[h] = lax.fori_loop(
                0, n - 1, lambda s, total: total + rs_in[h, s].astype(F32),
                red_s[h, part(mine), :].astype(F32),
            ).astype(BF16)

            def step(i, carry):
                pltpu.make_async_remote_copy(
                    src_ref=ag_src.at[h], dst_ref=ag_in.at[h, part(mine), :],
                    send_sem=ag_send.at[h], recv_sem=ag_recv.at[h],
                    device_id={"sp": lax.rem(me + i, n)},
                ).start()
                return carry

            lax.fori_loop(1, n, step, 0)

    for h in range(rounds):
        taps_round(h)
        scatter(h)

    def back_far(j):
        spread(d_s, da_s, j, 0, far, far + edge)
        correlate(da_s, x_s, j, 0, far, backward)

    def back_near(j):
        spread(d_s, db_s, j, rows - BLOCK, near, near + edge)
        correlate(db_s, x_s, j, rows - BLOCK, near, backward)

    def outputs(b):
        at = pl.ds(b * BLOCK, BLOCK)

        def run(j):
            sig = jax.nn.sigmoid(g_ref[at, cols(j)].astype(F32))
            first = x_s[j, at, :] * sig
            ag_ref[at, cols(j)] = first.astype(BF16)
            gg_ref[at, cols(j)] = (first * a_ref[at, cols(j)].astype(F32) * (1.0 - sig)).astype(BF16)

        each_tile(run)

    each_tile(back_far)
    for b in range(blocks - 1):
        outputs(b)
    for h in range(rounds):
        gather(h)

    @pl.when(me < n - 1)
    def _():
        dc_copy.wait_recv()

        def widen(j):
            d_s[j, pl.ds(rows, HALO), :] = dc_in[j].astype(F32)

        each_tile(widen)

    @pl.when(me == n - 1)
    def _():
        def clear(j):
            d_s[j, pl.ds(rows, HALO), :] = jnp.zeros((HALO, LANES), F32)

        each_tile(clear)

    each_tile(back_near)
    outputs(blocks - 1)

    @pl.when(me < n - 1)
    def _():
        glu_copy.wait_send()

    @pl.when(me > 0)
    def _():
        dc_copy.wait_send()

    for i in range(2 * blocks):
        stat_copy(i).wait_send()

    for h in range(rounds):
        @pl.when(owner)
        def _():
            bytes_of(rs_in.at[h], ag_send.at[h]).wait()
            if owners > 1:
                rest = pl.ds(0, (owners - 1) * chunk)
                bytes_of(red_s.at[h, rest, :], rs_send.at[h]).wait()
                bytes_of(ag_in.at[h, rest, :], ag_recv.at[h]).wait()
            ag_in[h, part(mine), :] = ag_src[h]

        @pl.when(jnp.logical_not(owner))
        def _():
            bytes_of(red_s.at[h], rs_send.at[h]).wait()
            bytes_of(ag_in.at[h], ag_recv.at[h]).wait()

        sums_ref[h] = ag_in[h].astype(F32)


def finish(
    width, slots, part_tiles,
    ag_ref, gg_ref, sums_ref,
    ag_out, gg_out, tg_out, gaing_out, shiftg_out,
    tg_ref, gaing_ref, shiftg_ref, sems,
):
    copies = [
        pltpu.make_async_copy(src, dst, sems.at[i])
        for i, (src, dst) in enumerate((
            (ag_ref, ag_out), (gg_ref, gg_out), (tg_ref, tg_out),
            (gaing_ref, gaing_out), (shiftg_ref, shiftg_out),
        ))
    ]
    copies[0].start()
    copies[1].start()
    for h in range(sums_ref.shape[0]):
        for i in range(part_tiles):
            at = pl.ds((h * part_tiles + i) * LANES, LANES)
            tg_ref[:, at] = sums_ref[h, pl.ds(i * slots, width), :]
            gaing_ref[at] = sums_ref[h, i * slots + width, :]
            shiftg_ref[at] = sums_ref[h, part_tiles * slots + i, :]
    for copy in copies[2:]:
        copy.start()
    for copy in copies:
        copy.wait()


def solution(mesh):
    n, ntp = mesh.shape["sp"], mesh.shape["tp"]

    def body(proj_a, proj_gate, taps, norm_gain, norm_shift, cotangent):
        rows, chans = proj_a.shape
        width = taps.shape[0]
        edge = width - 1
        tiles, rounds, slots, chunk, owners, _ = plan(chans, width, n)
        blocks = rows // BLOCK
        far, near = (rows - BLOCK) // PACK, BLOCK // PACK
        vmem = pl.BlockSpec(memory_space=pltpu.VMEM)
        hbm = pl.BlockSpec(memory_space=pltpu.HBM)
        wide = jax.ShapeDtypeStruct((rows, chans), BF16)
        a_grad, gate_grad, sums = pl.pallas_call(
            functools.partial(kernel, n, width, chans * ntp),
            out_shape=(wide, wide, jax.ShapeDtypeStruct((rounds, owners * chunk, LANES), F32)),
            in_specs=[hbm] * 6,
            out_specs=(vmem,) * 3,
            scratch_shapes=[
                pltpu.VMEM((rows, chans), BF16),
                pltpu.VMEM((rows, chans), BF16),
                pltpu.VMEM((rows, chans), BF16),
                pltpu.VMEM((width, chans), BF16),
                pltpu.VMEM((chans,), F32),
                pltpu.VMEM((chans,), F32),
                pltpu.VMEM((tiles, width, PACK, LANES), BF16),
                pltpu.VMEM((tiles, HALO + rows, LANES), F32),
                pltpu.VMEM((tiles, far + edge, PACK, LANES), BF16),
                pltpu.VMEM((tiles, near + edge, PACK, LANES), BF16),
                pltpu.VMEM((tiles, rows, LANES), F32),
                pltpu.VMEM((tiles, rows, LANES), F32),
                pltpu.VMEM((tiles, rows + HALO, LANES), F32),
                pltpu.VMEM((tiles, far + near, PACK, LANES), BF16),
                pltpu.VMEM((tiles, far + edge, PACK, LANES), BF16),
                pltpu.VMEM((tiles, near + edge, PACK, LANES), BF16),
                pltpu.VMEM((tiles, 3 * SUB, LANES), F32),
                pltpu.VMEM((slots * STEP, LANES), F32),
                pltpu.VMEM((tiles, HALO, LANES), BF16),
                pltpu.VMEM((tiles, HALO, LANES), BF16),
                pltpu.VMEM((tiles, HALO, LANES), BF16),
                pltpu.VMEM((tiles, HALO, LANES), BF16),
                pltpu.VMEM((2 * blocks, BLOCK, LANES), F32),
                pltpu.VMEM((2 * blocks, BLOCK, LANES), F32),
                pltpu.VMEM((rows, LANES), F32),
                pltpu.VMEM((owners * chunk, LANES), F32),
                pltpu.VMEM((rounds, owners * chunk, LANES), BF16),
                pltpu.VMEM((rounds, n - 1, chunk, LANES), BF16),
                pltpu.VMEM((rounds, chunk, LANES), BF16),
                pltpu.VMEM((rounds, owners * chunk, LANES), BF16),
                pltpu.SemaphoreType.DMA((6,)),
                pltpu.SemaphoreType.DMA((2,)),
                pltpu.SemaphoreType.DMA((2,)),
                pltpu.SemaphoreType.DMA((2 * blocks,)),
                pltpu.SemaphoreType.DMA((2 * blocks,)),
                pltpu.SemaphoreType.DMA((rounds,)),
                pltpu.SemaphoreType.DMA((rounds,)),
                pltpu.SemaphoreType.DMA((rounds,)),
                pltpu.SemaphoreType.DMA((rounds,)),
            ],
            compiler_params=pltpu.CompilerParams(
                collective_id=0, has_side_effects=True, vmem_limit_bytes=40 * 1024 * 1024
            ),
        )(*(
            pltpu.with_memory_space_constraint(x, pltpu.HBM)
            for x in (proj_a, proj_gate, taps, norm_gain, norm_shift, cotangent)
        ))
        vector = jax.ShapeDtypeStruct((chans,), F32)
        return pl.pallas_call(
            functools.partial(finish, width, slots, tiles // rounds),
            out_shape=(wide, wide, jax.ShapeDtypeStruct((width, chans), F32), vector, vector),
            in_specs=[vmem] * 3,
            out_specs=(hbm,) * 5,
            scratch_shapes=[
                pltpu.VMEM((width, chans), F32),
                pltpu.VMEM((chans,), F32),
                pltpu.VMEM((chans,), F32),
                pltpu.SemaphoreType.DMA((5,)),
            ],
            compiler_params=pltpu.CompilerParams(vmem_limit_bytes=16 * 1024 * 1024),
        )(a_grad, gate_grad, sums)

    placed = (P("sp", "tp"), P("sp", "tp"), P(None, "tp"), P("tp"), P("tp"), P("sp", "tp"))
    return jax.shard_map(
        body,
        mesh=mesh,
        in_specs=placed,
        out_specs=(P("sp", "tp"), P("sp", "tp"), P(None, "tp"), P("tp"), P("tp")),
        check_vma=False,
    )
```

time: 35.5 us -> 28.5 us (0.80)
  Pallas kernels: 34.6 us -> 27.7 us
    pallas_call x2, Pallas kernels: 34.6 us -> 27.7 us  [the longest x1 26.4 us: body(): pl.pallas_call(functools.partial(kernel, n, width, chans * ntp), out_shap...]
where the time goes in v1:
time: 28.5 us; the launch traced here: 28.3 us
  Pallas kernels  27.7 us (97%)
  between operations  0.64 us (2%)
    pallas_call x1, Pallas kernels, body(): pl.pallas_call(functools.partial(kernel, n, width, chans * ntp), out_shap...  26.4 us
    pallas_call x1, Pallas kernels, body(): pl.pallas_call(functools.partial(finish, width, slots, tiles // rounds),...  1.24 us

profile of v1, /device:TPU:0, one launch (start us, length us, event | category | flops | bytes accessed | tf_op | source)
XLA Modules:
  0.0 28.3 jit_solution(60424312532215533)
XLA Ops:
  0.6 26.4 %shard_map.101 = (bf16[256,1536]{1,0:T(8,128)(2,1)S(1)}, bf16[256,1536]{1,0:T(8,128)(2,1)S(1)}, f32[2,224,128]{2,1,0:T(8,128)S(1)}) custom-call(bf16[256,1536]{1,0:T(8,128)(2,1)} %a_hbm.1, bf16[256,1536]{1,0:T(8,128)(2,1)} %g_hbm.1, bf16[31,1536]{1,0:T(8,128)(2,1)} %taps_hbm.1, f32[1536]{0:T(1024)} %gain_hbm.1, f32[1536]{0:T(1024)} %shift_hbm.1, ...), custom_call_target="tpu_custom_call" | custom-call | tf_op jit(solution)/shard_map/pallas_call | solution.py:466
  27.1 1.2 %shard_map.102 = (bf16[256,1536]{1,0:T(8,128)(2,1)}, bf16[256,1536]{1,0:T(8,128)(2,1)}, f32[31,1536]{1,0:T(8,128)}, f32[1536]{0:T(1024)}, f32[1536]{0:T(1024)}) custom-call(bf16[256,1536]{1,0:T(8,128)(2,1)S(1)} %get-tuple-element.8.ag_ref, bf16[256,1536]{1,0:T(8,128)(2,1)S(1)} %get-tuple-element.9.gg_ref, f32[2,224,128]{2,1,0:T(8,128)S(1)} %get-tuple-element.10.sums_ref), custom_call_target="tpu_custom_call" | custom-call | tf_op jit(solution)/shard_map/pallas_call | solution.py:520

commit v2 on v1

--- a/solution.py
+++ b/solution.py
@@ -54,18 +54,18 @@
     lead = HALO - edge
     tiles, rounds, slots, chunk, owners, first_owner = plan(chans, width, n)
     part_tiles = tiles // rounds
-    blocks = rows // BLOCK
-    far, near = (rows - BLOCK) // PACK, BLOCK // PACK
+    far, near = (rows - HALO) // PACK, HALO // PACK
+    first_rows = (0, HALO)
+    late = ((HALO, BLOCK - HALO), *((b, BLOCK) for b in range(BLOCK, rows, BLOCK)))
+    parts = 2 if tiles % 2 == 0 else 1
+    split = tiles // parts
+    halves = [pl.ds(h * split * LANES, split * LANES) for h in range(parts)]
+    pieces = [(taps_hbm, taps_ref)]
+    for half in halves:
+        pieces += [(g_hbm.at[:, half], g_ref.at[:, half]), (a_hbm.at[:, half], a_ref.at[:, half])]
+    pieces += [(gain_hbm, gain_ref), (shift_hbm, shift_ref), (cot_hbm, cot_ref)]
     loads = [
-        pltpu.make_async_copy(src, dst, in_sem.at[i])
-        for i, (src, dst) in enumerate((
-            (taps_hbm, taps_ref),
-            (g_hbm, g_ref),
-            (a_hbm, a_ref),
-            (gain_hbm, gain_ref),
-            (shift_hbm, shift_ref),
-            (cot_hbm, cot_ref),
-        ))
+        pltpu.make_async_copy(src, dst, in_sem.at[i]) for i, (src, dst) in enumerate(pieces)
     ]
     for load in loads:
         load.start()
@@ -110,9 +110,9 @@
         device_id={"sp": lax.rem(me + n - 1, n)},
     )
 
-    def spread(src, dst, j, base, stride, count, at=0):
+    def spread(src, dst, j, base, stride, count):
         for m in range(count):
-            dst[j, at + m] = src[j, pl.ds(base + m, PACK, stride=stride), :].astype(BF16)
+            dst[j, m] = src[j, pl.ds(base + m, PACK, stride=stride), :].astype(BF16)
 
     def correlate(src, dst, j, base, stride, order):
         for m in range(stride):
@@ -129,67 +129,90 @@
             tap_s[j, k] = jnp.broadcast_to(row, (PACK, LANES)).astype(BF16)
 
     def gate_tile(j):
-        for b in range(blocks):
-            at = pl.ds(b * BLOCK, BLOCK)
+        for base, size in (first_rows, *late):
+            at = pl.ds(base, size)
             a = a_ref[at, cols(j)].astype(F32)
             g = g_ref[at, cols(j)].astype(F32)
-            glu = (a * jax.nn.sigmoid(g)).astype(BF16)
-            x_s[j, pl.ds(HALO + b * BLOCK, BLOCK), :] = glu.astype(F32)
-            if b == blocks - 1:
-                glu_out[j] = glu[BLOCK - HALO :]
-        spread(x_s, xa_s, j, lead + BLOCK, far, far + edge)
+            glu = a * jax.nn.sigmoid(g)
+            if base == 0:
+                glu = glu.astype(BF16).astype(F32)
+            x_s[j, pl.ds(HALO + base, size), :] = glu
+            if base + size == rows:
+                glu_out[j] = glu[size - HALO :].astype(BF16)
+
+    def far_tile(j):
+        spread(x_s, xa_s, j, lead + HALO, far, far + edge)
+
+    def gate_next(j, carry):
+        far_tile(j - 1)
+        gate_tile(j)
+        return carry
 
     loads[0].wait()
     each_tile(spread_taps)
-    loads[1].wait()
-    loads[2].wait()
-    each_tile(gate_tile)
+    for h in range(parts):
+        loads[1 + 2 * h].wait()
+        loads[2 + 2 * h].wait()
+        if h == 0:
+            gate_tile(0)
+        lax.fori_loop(max(h * split, 1), (h + 1) * split, gate_next, 0)
+    far_tile(tiles - 1)
     pl.semaphore_wait(barrier, n)
 
     @pl.when(me < n - 1)
     def _():
         glu_copy.start()
 
-    each_tile(lambda j: correlate(xa_s, conv_s, j, BLOCK, far, forward))
-
-    lane = lax.broadcasted_iota(jnp.int32, (BLOCK, LANES), 1)
-    zero = jnp.zeros((BLOCK, LANES), F32)
-
-    def stat_copy(i):
+    each_tile(lambda j: correlate(xa_s, conv_s, j, HALO, far, forward))
+
+    def stat_copy(phase, rows_of):
+        at = pl.ds(*rows_of)
         return pltpu.make_async_remote_copy(
-            src_ref=st_out.at[i], dst_ref=st_in.at[i], send_sem=st_send.at[i],
-            recv_sem=st_recv.at[i], device_id={"tp": other},
+            src_ref=st_out.at[phase, :, at, :], dst_ref=st_in.at[phase, :, at, :],
+            send_sem=st_send.at[0],
+            recv_sem=st_recv.at[phase, ((0, HALO), *late).index(rows_of)],
+            device_id={"tp": other},
         )
 
-    def send_stats(i, first, second):
-        first = jnp.sum(first, axis=1, keepdims=True)
-        second = jnp.sum(second, axis=1, keepdims=True)
-        st_out[i] = jnp.where(lane < LANES // 2, first, second)
-        stat_copy(i).start()
-
-    def both_stats(i):
-        stat_copy(i).wait_recv()
-        both = (st_out[i] + st_in[i]) * (1.0 / full)
-        first = jnp.broadcast_to(both[:, 0:1], (BLOCK, LANES))
-        second = jnp.broadcast_to(both[:, LANES // 2 : LANES // 2 + 1], (BLOCK, LANES))
-        return first, second
-
-    def moments(b):
+    def send_stats(phase, rows_of, first, second):
+        st_out[phase, 0, pl.ds(*rows_of), :] = first
+        st_out[phase, 1, pl.ds(*rows_of), :] = second
+        stat_copy(phase, rows_of).start()
+
+    def both_stats(group, phase):
+        for rows_of in group:
+            stat_copy(phase, rows_of).wait_recv()
+        for rows_of in group:
+            at = pl.ds(*rows_of)
+            both = (st_out[phase, :, at, :] + st_in[phase, :, at, :]) * (1.0 / full)
+            first, second = (
+                jnp.broadcast_to(jnp.sum(both[q], axis=1, keepdims=True), both[q].shape)
+                for q in range(2)
+            )
+            if phase == 0:
+                second = lax.rsqrt(jnp.maximum(second - first * first, 0.0) + EPS)
+            stat_s[2 * phase, at, :] = first
+            stat_s[2 * phase + 1, at, :] = second
+
+    def zeros(rows_of):
+        zero = jnp.zeros((rows_of[1], LANES), F32)
+        return zero, zero
+
+    def moments(rows_of):
         def step(j, carry):
             first, second = carry
-            x = conv_s[j, pl.ds(b * BLOCK, BLOCK), :]
+            x = conv_s[j, pl.ds(*rows_of), :]
             return first + x, second + x * x
 
-        send_stats(b, *over_tiles(step, (zero, zero), 3))
+        send_stats(0, rows_of, *over_tiles(step, zeros(rows_of), 3))
 
     def fold(x):
         return jnp.sum(x.reshape(x.shape[0] // SUB, SUB, LANES), axis=0)
 
-    def normalise(b):
-        at = pl.ds(b * BLOCK, BLOCK)
-        mean, square = both_stats(b)
-        rstd = lax.rsqrt(jnp.maximum(square - mean * mean, 0.0) + EPS)
-        stat_s[at, :] = rstd
+    def normalise(rows_of):
+        at = pl.ds(*rows_of)
+        mean = stat_s[0, at, :]
+        rstd = stat_s[1, at, :]
 
         def step(j, carry):
             first, second = carry
@@ -205,12 +228,13 @@
             dn_s[j, at, :] = dn
             return first + dn, second + dn * normed
 
-        send_stats(blocks + b, *lax.fori_loop(0, tiles, step, (zero, zero)))
-
-    def dconv(b):
-        at = pl.ds(b * BLOCK, BLOCK)
-        first, second = both_stats(blocks + b)
-        rstd = stat_s[at, :]
+        send_stats(1, rows_of, *over_tiles(step, zeros(rows_of), 1))
+
+    def dconv(rows_of):
+        at = pl.ds(*rows_of)
+        rstd = stat_s[1, at, :]
+        first = stat_s[2, at, :]
+        second = stat_s[3, at, :]
 
         def step(j, carry):
             d_s[j, at, :] = rstd * (dn_s[j, at, :] - first - conv_s[j, at, :] * second)
@@ -218,19 +242,25 @@
 
         over_tiles(step, 0, 2)
 
-    for b in range(1, blocks):
+    for b in late:
         moments(b)
 
-    loads[3].wait()
-    loads[4].wait()
+    loads[-3].wait()
+    loads[-2].wait()
 
     def parameters(j):
         par_s[j, 0:1, :] = gain_ref[cols(j)].reshape(1, LANES)
         par_s[j, 1:2, :] = shift_ref[cols(j)].reshape(1, LANES)
         par_s[j, pl.ds(SUB, 2 * SUB), :] = jnp.zeros((2 * SUB, LANES), F32)
+        part_s[j, pl.ds(width * STEP, (slots - width) * STEP), :] = jnp.zeros(
+            ((slots - width) * STEP, LANES), F32
+        )
 
     each_tile(parameters)
-    loads[5].wait()
+    loads[-1].wait()
+    both_stats(late, 0)
+    for b in late:
+        normalise(b)
 
     @pl.when(me > 0)
     def _():
@@ -253,43 +283,38 @@
         correlate(xb_s, conv_s, j, 0, near, forward)
 
     each_tile(near_tile)
-    moments(0)
-    order = (*range(1, blocks), 0)
-    for b in order:
-        normalise(b)
-    for b in order:
+    moments(first_rows)
+    both_stats(late, 1)
+    for b in late:
         dconv(b)
 
-    def head(j):
-        dc_out[j] = d_s[j, pl.ds(0, HALO), :].astype(BF16)
-
-    each_tile(head)
-
-    @pl.when(me > 0)
-    def _():
-        dc_copy.start()
-
-    spare = owners * chunk - part_tiles * (slots + 1)
-    part_s[pl.ds(width * STEP, (slots - width) * STEP), :] = jnp.zeros(
-        ((slots - width) * STEP, LANES), F32
-    )
-
-    def taps_round(h):
+    def taps_far(h):
         def step(i, carry):
             j = h * part_tiles + i
-            spread(d_s, d_t, j, BLOCK, far, far)
-            spread(d_s, d_t, j, 0, near, near, far)
+            spread(d_s, d_t, j, HALO, far, far)
             for k in range(width):
-                both = products(
-                    [(xa_s[j, m + k], d_t[j, m]) for m in range(far)]
-                    + [(xb_s[j, m + k], d_t[j, far + m]) for m in range(near)]
-                )
-                part_s[pl.ds(k * STEP, SUB), :] = both[:SUB] + both[SUB:]
-            part_s[pl.ds(width * STEP, SUB), :] = par_s[j, pl.ds(SUB, SUB), :]
+                both = products((xa_s[j, m + k], d_t[j, m]) for m in range(far))
+                part_s[j, pl.ds(k * STEP, SUB), :] = both[:SUB] + both[SUB:]
+            return carry
+
+        lax.fori_loop(0, part_tiles, step, 0)
+
+    spare = owners * chunk - part_tiles * (slots + 1)
+
+    def taps_near(h):
+        def step(i, carry):
+            j = h * part_tiles + i
+            d = [d_s[j, pl.ds(r, SUB), :] for r in range(0, HALO, SUB)]
+            for k in range(width):
+                total = part_s[j, pl.ds(k * STEP, SUB), :]
+                for r in range(0, HALO, SUB):
+                    total = total + d[r // SUB] * x_s[j, pl.ds(lead + k + r, SUB), :]
+                part_s[j, pl.ds(k * STEP, SUB), :] = total
+            part_s[j, pl.ds(width * STEP, SUB), :] = par_s[j, pl.ds(SUB, SUB), :]
             for q in range(slots // SUB):
-                total = part_s[pl.ds(q * SUB * STEP, SUB, stride=STEP), :]
+                total = part_s[j, pl.ds(q * SUB * STEP, SUB, stride=STEP), :]
                 for r in range(1, SUB):
-                    total = total + part_s[pl.ds(q * SUB * STEP + r, SUB, stride=STEP), :]
+                    total = total + part_s[j, pl.ds(q * SUB * STEP + r, SUB, stride=STEP), :]
                 red_f[pl.ds(pl.multiple_of(i * slots, SUB) + q * SUB, SUB), :] = total
             red_f[pl.ds(part_tiles * slots + i, 1), :] = jnp.sum(
                 par_s[j, pl.ds(2 * SUB, SUB), :], axis=0, keepdims=True
@@ -300,6 +325,14 @@
         if spare:
             red_f[pl.ds(part_tiles * (slots + 1), spare), :] = jnp.zeros((spare, LANES), F32)
         red_s[h] = red_f[...].astype(BF16)
+
+    taps_far(0)
+    both_stats((first_rows,), 0)
+    normalise(first_rows)
+    for h in range(1, rounds):
+        taps_far(h)
+    both_stats((first_rows,), 1)
+    dconv(first_rows)
 
     mine = me - first_owner
     owner = jnp.logical_and(mine >= 0, mine < owners)
@@ -347,7 +380,7 @@
             lax.fori_loop(1, n, step, 0)
 
     for h in range(rounds):
-        taps_round(h)
+        taps_near(h)
         scatter(h)
 
     def back_far(j):
@@ -355,11 +388,11 @@
         correlate(da_s, x_s, j, 0, far, backward)
 
     def back_near(j):
-        spread(d_s, db_s, j, rows - BLOCK, near, near + edge)
-        correlate(db_s, x_s, j, rows - BLOCK, near, backward)
-
-    def outputs(b):
-        at = pl.ds(b * BLOCK, BLOCK)
+        spread(d_s, db_s, j, rows - HALO, near, near + edge)
+        correlate(db_s, x_s, j, rows - HALO, near, backward)
+
+    def outputs(rows_of):
+        at = pl.ds(*rows_of)
 
         def run(j):
             sig = jax.nn.sigmoid(g_ref[at, cols(j)].astype(F32))
@@ -369,9 +402,18 @@
 
         each_tile(run)
 
+    def head(j):
+        dc_out[j] = d_s[j, pl.ds(0, HALO), :].astype(BF16)
+
+    each_tile(head)
     each_tile(back_far)
-    for b in range(blocks - 1):
-        outputs(b)
+    for b in range(0, rows - HALO, BLOCK):
+        outputs((b, min(BLOCK, rows - HALO - b)))
+
+    @pl.when(me > 0)
+    def _():
+        dc_copy.start()
+
     for h in range(rounds):
         gather(h)
 
@@ -392,7 +434,7 @@
         each_tile(clear)
 
     each_tile(back_near)
-    outputs(blocks - 1)
+    outputs((rows - HALO, HALO))
 
     @pl.when(me < n - 1)
     def _():
@@ -402,8 +444,7 @@
     def _():
         dc_copy.wait_send()
 
-    for i in range(2 * blocks):
-        stat_copy(i).wait_send()
+    bytes_of(stat_s, st_send.at[0]).wait()
 
     for h in range(rounds):
         @pl.when(owner)
@@ -458,8 +499,8 @@
         width = taps.shape[0]
         edge = width - 1
         tiles, rounds, slots, chunk, owners, _ = plan(chans, width, n)
-        blocks = rows // BLOCK
-        far, near = (rows - BLOCK) // PACK, BLOCK // PACK
+        blocks = 1 + rows // BLOCK
+        far, near = (rows - HALO) // PACK, HALO // PACK
         vmem = pl.BlockSpec(memory_space=pltpu.VMEM)
         hbm = pl.BlockSpec(memory_space=pltpu.HBM)
         wide = jax.ShapeDtypeStruct((rows, chans), BF16)
@@ -482,28 +523,28 @@
                 pltpu.VMEM((tiles, rows, LANES), F32),
                 pltpu.VMEM((tiles, rows, LANES), F32),
                 pltpu.VMEM((tiles, rows + HALO, LANES), F32),
-                pltpu.VMEM((tiles, far + near, PACK, LANES), BF16),
+                pltpu.VMEM((tiles, far, PACK, LANES), BF16),
                 pltpu.VMEM((tiles, far + edge, PACK, LANES), BF16),
                 pltpu.VMEM((tiles, near + edge, PACK, LANES), BF16),
                 pltpu.VMEM((tiles, 3 * SUB, LANES), F32),
-                pltpu.VMEM((slots * STEP, LANES), F32),
+                pltpu.VMEM((tiles, slots * STEP, LANES), F32),
                 pltpu.VMEM((tiles, HALO, LANES), BF16),
                 pltpu.VMEM((tiles, HALO, LANES), BF16),
                 pltpu.VMEM((tiles, HALO, LANES), BF16),
                 pltpu.VMEM((tiles, HALO, LANES), BF16),
-                pltpu.VMEM((2 * blocks, BLOCK, LANES), F32),
-                pltpu.VMEM((2 * blocks, BLOCK, LANES), F32),
-                pltpu.VMEM((rows, LANES), F32),
+                pltpu.VMEM((2, 2, rows, LANES), F32),
+                pltpu.VMEM((2, 2, rows, LANES), F32),
+                pltpu.VMEM((4, rows, LANES), F32),
                 pltpu.VMEM((owners * chunk, LANES), F32),
                 pltpu.VMEM((rounds, owners * chunk, LANES), BF16),
                 pltpu.VMEM((rounds, n - 1, chunk, LANES), BF16),
                 pltpu.VMEM((rounds, chunk, LANES), BF16),
                 pltpu.VMEM((rounds, owners * chunk, LANES), BF16),
-                pltpu.SemaphoreType.DMA((6,)),
+                pltpu.SemaphoreType.DMA((8,)),
                 pltpu.SemaphoreType.DMA((2,)),
                 pltpu.SemaphoreType.DMA((2,)),
-                pltpu.SemaphoreType.DMA((2 * blocks,)),
-                pltpu.SemaphoreType.DMA((2 * blocks,)),
+                pltpu.SemaphoreType.DMA((1,)),
+                pltpu.SemaphoreType.DMA((2, blocks)),
                 pltpu.SemaphoreType.DMA((rounds,)),
                 pltpu.SemaphoreType.DMA((rounds,)),
                 pltpu.SemaphoreType.DMA((rounds,)),

time: 28.5 us -> 26.3 us (0.923)
  Pallas kernels: 27.7 us -> 25.5 us
    pallas_call x1, Pallas kernels: 26.4 us -> 24.3 us  [body(): pl.pallas_call(functools.partial(kernel, n, width, chans * ntp), out_shap...]
where the time goes in v2:
time: 26.3 us; the launch traced here: 26.2 us
  Pallas kernels  25.5 us (97%)
  between operations  0.64 us (2%)
    pallas_call x1, Pallas kernels, body(): pl.pallas_call(functools.partial(kernel, n, width, chans * ntp), out_shap...  24.3 us
    pallas_call x1, Pallas kernels, body(): pl.pallas_call(functools.partial(finish, width, slots, tiles // rounds),...  1.24 us

profile of v2, /device:TPU:0, one launch (start us, length us, event | category | flops | bytes accessed | tf_op | source)
XLA Modules:
  0.0 26.2 jit_solution(4320516289391730877)
XLA Ops:
  0.6 24.3 %shard_map.101 = (bf16[256,1536]{1,0:T(8,128)(2,1)S(1)}, bf16[256,1536]{1,0:T(8,128)(2,1)S(1)}, f32[2,224,128]{2,1,0:T(8,128)S(1)}) custom-call(bf16[256,1536]{1,0:T(8,128)(2,1)} %a_hbm.1, bf16[256,1536]{1,0:T(8,128)(2,1)} %g_hbm.1, bf16[31,1536]{1,0:T(8,128)(2,1)} %taps_hbm.1, f32[1536]{0:T(1024)} %gain_hbm.1, f32[1536]{0:T(1024)} %shift_hbm.1, ...), custom_call_target="tpu_custom_call" | custom-call | tf_op jit(solution)/shard_map/pallas_call | solution.py:507
  24.9 1.2 %shard_map.102 = (bf16[256,1536]{1,0:T(8,128)(2,1)}, bf16[256,1536]{1,0:T(8,128)(2,1)}, f32[31,1536]{1,0:T(8,128)}, f32[1536]{0:T(1024)}, f32[1536]{0:T(1024)}) custom-call(bf16[256,1536]{1,0:T(8,128)(2,1)S(1)} %get-tuple-element.8.ag_ref, bf16[256,1536]{1,0:T(8,128)(2,1)S(1)} %get-tuple-element.9.gg_ref, f32[2,224,128]{2,1,0:T(8,128)S(1)} %get-tuple-element.10.sums_ref), custom_call_target="tpu_custom_call" | custom-call | tf_op jit(solution)/shard_map/pallas_call | solution.py:561
